TPU v7x, 256 devices: a whole 4x4x8 slice. The times are simulated.
256 devices in a mesh: sp: 32 (over z, y), tp: 8 (over x, core).
Axes of the slice: x: 4, y: 4, z: 8, core: 2. Of those that a mesh axis runs over, the one named last changes fastest.
Arguments:
- inputs: bfloat16 [16384, 2048], P('sp', 'tp'), may hold values from -6 to 6
- norm_gain: float32 [2048], replicated, may hold values from 0.1 to 1.9
- latent_query: bfloat16 [2048, 1536], P(None, 'tp'), may hold values from -2 to 2
- latent_down: bfloat16 [2048, 512], replicated, may hold values from -2 to 2
- rope_down: bfloat16 [2048, 32], replicated, may hold values from -2 to 2
- latent_gain: float32 [512], replicated, may hold values from 0.1 to 1.9
- latent_up: bfloat16 [512, 2048], P(None, 'tp'), may hold values from -2 to 2
- window_query: bfloat16 [2048, 1024], P(None, 'tp'), may hold values from -2 to 2
- window_key: bfloat16 [2048, 512], P(None, 'tp'), may hold values from -2 to 2
- window_value: bfloat16 [2048, 512], P(None, 'tp'), may hold values from -0.125 to 0.125
- sink_logit: float32 [16], P('tp'), may hold values from 3 to 8
- out_latent: bfloat16 [1024, 2048], P('tp'), may hold values from -0.1875 to 0.1875
- out_window: bfloat16 [1024, 2048], P('tp'), may hold values from -0.1875 to 0.1875
Outputs:
- attended: bfloat16 [16384, 2048], P('sp', 'tp')
All inputs are finite; a program needn't handle non-finite values.
Results may differ from a plain program's by a relative error of at most 0.017.
Values may be sent and summed in bfloat16 or wider, within the bound.
No kernel may reach another device: no remote copies, remote signals or barrier semaphores. Data moves between devices by JAX's collectives and lax.ppermute only.
A program may use at most 128 MiB of HBM per device.

v0:
```python
import jax
import jax.numpy as jnp
from jax import lax
from jax.sharding import PartitionSpec as P

NOPE = 64
ROPE = 32
HEAD = 64
WINDOW = 128


epsilon = 1e-06
key_block = 512


def sent_to_all(value, axis):
    peers = lax.axis_size(axis)
    return lax.all_to_all(
        jnp.broadcast_to(value[None], (peers, *value.shape)), axis, 0, 0, tiled=True
    )


def in_order(parts, dim):
    parts = jnp.moveaxis(parts, 0, dim)
    shape = parts.shape
    return parts.reshape(*shape[:dim], shape[dim] * shape[dim + 1], *shape[dim + 2 :])


def gather_directly(value, axis, dim):
    parts = sent_to_all(value, axis)
    return in_order(parts, dim)


def sent_together(arrays, axis, dim, along):
    ends, at = ([], 0)
    for a in arrays[:-1]:
        at += a.shape[along]
        ends.append(at)
    both = jnp.concatenate(arrays, axis=along)
    return tuple(jnp.split(lax.all_gather(both, axis, axis=dim, tiled=True), ends, axis=along))


def with_halo(cells, sides, width):
    for axis, dim in sides:
        count = lax.axis_size(axis)
        ends = count - 1
        head = lax.slice_in_dim(cells, 0, width, axis=dim)
        tail = lax.slice_in_dim(cells, cells.shape[dim] - width, cells.shape[dim], axis=dim)
        cells = jnp.concatenate(
            [
                lax.ppermute(tail, axis, [(i, (i + 1) % count) for i in range(ends)]),
                cells,
                lax.ppermute(head, axis, [((i + 1) % count, i) for i in range(ends)]),
            ],
            axis=dim,
        )
    return cells


def in_blocks(value, dim, peers):
    shape = value.shape
    parts = value.reshape(*shape[:dim], peers, shape[dim] // peers, *shape[dim + 1 :])
    return jnp.moveaxis(parts, dim, 0)


def summed_on_arrival(value, axis, dim):
    parts = in_blocks(value, dim, lax.axis_size(axis))
    arrived = lax.all_to_all(parts, axis, split_axis=0, concat_axis=0, tiled=True)
    return arrived.astype(jnp.float32).sum(axis=0)


def rms_scale(values, gains):
    return values * lax.rsqrt(jnp.mean(values * values, axis=-1, keepdims=True) + epsilon) * gains


def rotary(values, positions):
    half_width = values.shape[-1] // 2
    inverse = 1.0 / 10000.0 ** (
        jnp.arange(0, 2 * half_width, 2).astype(jnp.float32) / (2 * half_width)
    )
    angles = positions[:, None] * inverse[None, :]
    cosine_table = jnp.cos(angles)[:, None, :]
    sine_table = jnp.sin(angles)[:, None, :]
    first_half = values[..., :half_width]
    second_half = values[..., half_width:]
    return jnp.concatenate(
        [
            first_half * cosine_table - second_half * sine_table,
            second_half * cosine_table + first_half * sine_table,
        ],
        axis=-1,
    )


def attend(running, queries, key_data, rope_keys):
    maxima, denoms, totals = running
    head_count = queries.shape[1]
    stacked = key_data.reshape(key_data.shape[0], head_count, NOPE + HEAD)
    scores = jnp.einsum(
        "qhn,khn->hqk", queries[..., :NOPE], stacked[..., :NOPE], preferred_element_type=jnp.float32
    )
    scores = scores + jnp.einsum(
        "qhr,kr->hqk", queries[..., NOPE:], rope_keys, preferred_element_type=jnp.float32
    )
    scores = scores * (NOPE + ROPE) ** (-0.5)
    highest = jnp.maximum(maxima, jnp.max(scores, axis=-1))
    weights = jnp.exp(scores - highest[..., None])
    shrink = jnp.exp(maxima - highest)
    denoms = denoms * shrink + jnp.sum(weights, axis=-1)
    totals = totals * jnp.transpose(shrink)[:, :, None] + jnp.einsum(
        "hqk,khd->qhd",
        weights.astype(jnp.bfloat16),
        stacked[..., NOPE:],
        preferred_element_type=jnp.float32,
    )
    return (highest, denoms, totals)


def attend_rows(running, queries, key_data, rope_keys):
    row_total = key_data.shape[0]

    def advance(state_now, pieces):
        return (attend(state_now, queries, pieces[0], pieces[1]), None)

    sliced = (
        key_data.reshape(row_total // key_block, key_block, key_data.shape[1]),
        rope_keys.reshape(row_total // key_block, key_block, rope_keys.shape[1]),
    )
    running, unused = lax.scan(advance, running, sliced)
    return running


def shards(
    inputs,
    norm_gain,
    latent_query,
    latent_down,
    rope_down,
    latent_gain,
    latent_up,
    window_query,
    window_key,
    window_value,
    sink_logit,
    out_latent,
    out_window,
):
    row_count = inputs.shape[0]
    gathered = gather_directly(inputs, "tp", 1)
    hidden = rms_scale(gathered.astype(jnp.float32), norm_gain).astype(jnp.bfloat16)
    offset = lax.axis_index("sp") * row_count
    length_all = row_count * lax.axis_size("sp")
    positions = (offset + jnp.arange(row_count)).astype(jnp.float32)
    latent = rms_scale(
        jnp.dot(hidden, latent_down, preferred_element_type=jnp.float32), latent_gain
    ).astype(jnp.bfloat16)
    shared = rotary(
        jnp.dot(hidden, rope_down, preferred_element_type=jnp.float32)[:, None, :], positions
    )[:, 0, :].astype(jnp.bfloat16)
    head_count = latent_up.shape[1] // (NOPE + HEAD)
    queries = jnp.dot(hidden, latent_query, preferred_element_type=jnp.float32).reshape(
        row_count, head_count, NOPE + ROPE
    )
    queries = jnp.concatenate(
        [queries[..., :NOPE], rotary(queries[..., NOPE:], positions)], axis=-1
    ).astype(jnp.bfloat16)
    start_state = (
        jnp.full((head_count, row_count), -jnp.inf, jnp.float32),
        jnp.zeros((head_count, row_count), jnp.float32),
        jnp.zeros((row_count, head_count, HEAD), jnp.float32),
    )
    expanded = jnp.dot(latent, latent_up, preferred_element_type=jnp.float32).astype(jnp.bfloat16)
    pieces = sent_together((expanded, shared), "sp", 0, 1)
    maxima, denoms, totals = attend_rows(start_state, queries, pieces[0], pieces[1])
    latent_out = (
        (totals / jnp.transpose(denoms)[:, :, None])
        .reshape(row_count, head_count * HEAD)
        .astype(jnp.bfloat16)
    )
    window_heads = window_query.shape[1] // HEAD
    key_heads = window_key.shape[1] // HEAD
    group_size = window_heads // key_heads
    window_queries = rotary(
        jnp.dot(hidden, window_query, preferred_element_type=jnp.float32).reshape(
            row_count, window_heads, HEAD
        ),
        positions,
    ).astype(jnp.bfloat16)
    window_keys = rotary(
        jnp.dot(hidden, window_key, preferred_element_type=jnp.float32).reshape(
            row_count, key_heads, HEAD
        ),
        positions,
    ).astype(jnp.bfloat16)
    window_values = jnp.dot(hidden, window_value, preferred_element_type=jnp.float32).astype(
        jnp.bfloat16
    )
    packed = jnp.concatenate(
        [window_keys.reshape(row_count, key_heads * HEAD), window_values], axis=1
    )
    padded = with_halo(packed, (("sp", 0),), WINDOW)
    block_count = row_count // WINDOW
    grid_rows = padded.reshape(block_count + 2, WINDOW, packed.shape[1])
    banded = jnp.concatenate([grid_rows[:-2], grid_rows[1:-1], grid_rows[2:]], axis=1)
    band_keys = banded[..., : key_heads * HEAD].reshape(block_count, 3 * WINDOW, key_heads, HEAD)
    band_values = banded[..., key_heads * HEAD :].reshape(block_count, 3 * WINDOW, key_heads, HEAD)
    query_band = window_queries.reshape(block_count, WINDOW, key_heads, group_size, HEAD)
    scores = jnp.einsum(
        "nqhgd,nkhd->nhgqk", query_band, band_keys, preferred_element_type=jnp.float32
    ) * HEAD ** (-0.5)
    offsets = jnp.arange(3 * WINDOW)[None, :] - jnp.arange(WINDOW)[:, None]
    key_pos = (
        offset
        - WINDOW
        + jnp.arange(block_count)[:, None] * WINDOW
        + jnp.arange(3 * WINDOW)[None, :]
    )
    allowed = ((offsets >= 0) & (offsets <= 2 * WINDOW))[None] & (
        (key_pos >= 0) & (key_pos < length_all)
    )[:, None, :]
    scores = jnp.where(allowed[:, None, None], scores, -jnp.inf)
    sink_table = sink_logit.reshape(key_heads, group_size)[None, :, :, None]
    highest = jnp.maximum(jnp.max(scores, axis=-1), sink_table)
    weights = jnp.exp(scores - highest[..., None])
    denominators = jnp.sum(weights, axis=-1) + jnp.exp(sink_table - highest)
    window_mix = jnp.einsum(
        "nhgqk,nkhd->nqhgd",
        weights.astype(jnp.bfloat16),
        band_values,
        preferred_element_type=jnp.float32,
    )
    window_out = (
        (window_mix / jnp.transpose(denominators, (0, 3, 1, 2))[..., None])
        .reshape(row_count, window_heads * HEAD)
        .astype(jnp.bfloat16)
    )
    contract_dims = (((0,), (1,)), ((), ()))
    own_rows = summed_on_arrival(
        (
            lax.dot_general(
                out_latent, latent_out, contract_dims, preferred_element_type=jnp.float32
            )
            + lax.dot_general(
                out_window, window_out, contract_dims, preferred_element_type=jnp.float32
            )
        ).astype(jnp.bfloat16),
        "tp",
        0,
    )
    return jnp.transpose(own_rows).astype(jnp.bfloat16)


def solution(mesh):
    in_specs = (
        P("sp", "tp"),
        P(),
        P(None, "tp"),
        P(),
        P(),
        P(),
        P(None, "tp"),
        P(None, "tp"),
        P(None, "tp"),
        P(None, "tp"),
        P("tp"),
        P("tp", None),
        P("tp", None),
    )
    out_specs = P("sp", "tp")
    return jax.shard_map(shards, mesh=mesh, in_specs=in_specs, out_specs=out_specs, check_vma=False)
```

profile of v0, /device:TPU:1, one launch (start us, length us, event | category | flops | bytes accessed | tf_op | source)
XLA Modules:
  0.0 310.3 jit_solution(14386173593540342198)
XLA Ops:
  6.5 2.5 broadcast_in_dim.21
  9.1 7.4 %all-to-all-start = ((bf16[8,512,256]{2,1,0:T(8,128)(2,1)}), bf16[8,512,256]{2,1,0:T(8,128)(2,1)}, u32[]{:S(2)}, u32[]{:S(2)}) async-start(bf16[8,512,256]{2,1,0:T(8,128)(2,1)} %broadcast_in_dim.21), calls=%async_computation | async-start | bytes 4194304 | tf_op jit(solution)/shard_map/all_to_all | solution.py:18
  16.5 26.3 %all-to-all-done = bf16[8,512,256]{2,1,0:T(8,128)(2,1)} async-done(((bf16[8,512,256]{2,1,0:T(8,128)(2,1)}), bf16[8,512,256]{2,1,0:T(8,128)(2,1)}, u32[]{:S(2)}, u32[]{:S(2)}) %all-to-all-start) | async-done | bytes 2097184 | tf_op jit(solution)/shard_map/all_to_all | solution.py:18
  42.8 3.9 %copy.48 = bf16[8,512,256]{1,2,0:T(8,128)(2,1)} copy(bf16[8,512,256]{2,1,0:T(8,128)(2,1)} %all-to-all-done) | data formatting | bytes 4194304 | tf_op jit(solution)/shard_map/all_to_all | solution.py:18
  46.8 2.3 multiply_reduce_fusion
  50.4 1.3 multiply_reduce_fusion.1
  56.2 1.0 copy-done.3
  58.5 1.3 collective-permute-start.1
  59.8 4.2 %collective-permute-start = (bf16[128,128]{0,1:T(8,128)(2,1)S(1)}, bf16[128,128]{0,1:T(8,128)(2,1)S(1)}, u32[]{:S(2)}, u32[]{:S(2)}) collective-permute-start(bf16[128,128]{0,1:T(8,128)(2,1)S(1)} %get-tuple-element.125), channel_id=1, source_target_pairs={{0,8},{8,16},{16,24},{24,32},{32,40},{40,48},{48,56},{56,64},{64,7... | collective-permute-start | bytes 98312 | tf_op jit(solution)/shard_map/ppermute | solution.py:51
  66.4 91.0 %all-gather.2.cloned.1.call-done = bf16[16384,288]{0,1:T(8,128)(2,1)} async-done(((bf16[512,288]{0,1:T(8,128)(2,1)}), bf16[16384,288]{0,1:T(8,128)(2,1)}) %all-gather.2.cloned.1.call-update) | async-done | bytes 9437200 | tf_op jit(solution)/shard_map/all_gather | solution.py:40
  157.3 7.6 %split.8 = bf16[16384,256]{0,1:T(8,128)(2,1)} slice(bf16[16384,288]{0,1:T(8,128)(2,1)} %all-gather.2.cloned.1.call-done), slice={[0:16384], [0:256]} | slice | bytes 16777216 | tf_op jit(solution)/shard_map/split | solution.py:40
  164.9 7.8 %copy.91 = bf16[32,32,8,512]{3,2,0,1:T(8,128)(2,1)} copy(bf16[32,32,8,512]{3,2,1,0:T(8,128)(2,1)} %bitcast.159) | data formatting | bytes 16777216 | tf_op jit(solution)/shard_map/reshape | solution.py:126
  172.8 1.2 slice-done
  174.1 90.1 %while.15 = (s32[]{:T(128)}, f32[2,512]{1,0:T(2,128)S(1)}, f32[2,512]{1,0:T(2,128)S(1)}, f32[512,2,64]{0,2,1:T(8,128)S(1)}, bf16[32,512,256]{1,2,0:T(8,128)(2,1)...) while((s32[]{:T(128)}, f32[2,512]{1,0:T(2,128)S(1)}, ...), condition=%wide.region_5.6_spmd.clone, body=%wide.region_2.5_spmd.clone.sunk | while | flops 171644928 | bytes 12091513 | solution.py:129
  174.1 1.0 constant_dynamic-slice_fusion.2
  177.0 1.0 constant_dynamic-slice_fusion.2
  179.8 1.0 constant_dynamic-slice_fusion.2
  182.6 1.0 constant_dynamic-slice_fusion.2
  185.4 1.0 constant_dynamic-slice_fusion.2
  188.3 1.0 constant_dynamic-slice_fusion.2
  191.1 1.0 constant_dynamic-slice_fusion.2
  193.9 1.0 constant_dynamic-slice_fusion.2
  196.7 1.0 constant_dynamic-slice_fusion.2
  199.5 1.0 constant_dynamic-slice_fusion.2
  202.3 1.0 constant_dynamic-slice_fusion.2
  205.1 1.0 constant_dynamic-slice_fusion.2
  207.9 1.0 constant_dynamic-slice_fusion.2
  210.8 1.0 constant_dynamic-slice_fusion.2
  213.6 1.0 constant_dynamic-slice_fusion.2
  216.4 1.0 constant_dynamic-slice_fusion.2
  266.2 34.7 %all_to_all.10 = bf16[8,256,512]{1,2,0:T(8,128)(2,1)} all-to-all(bf16[8,256,512]{1,2,0:T(8,128)(2,1)S(1)} %bitcast.165), channel_id=1, replica_groups=mesh['sp'=32,'tp'=8] {'tp'}, dimensions={0} | all-to-all | bytes 4194304 | tf_op jit(solution)/shard_map/all_to_all | solution.py:68
  300.8 2.6 reduce_sum.54
  (328 shorter events, 83.9 us)
Async XLA Ops:
  6.5 43.9 %copy-start = (bf16[2048,512]{1,0:T(8,128)(2,1)S(1)}, bf16[2048,512]{1,0:T(8,128)(2,1)}, u32[]{:S(2)}) copy-start(bf16[2048,512]{1,0:T(8,128)(2,1)} %param.18) | copy-start | bytes 6291460
  9.1 33.7 %all-to-all-start = ((bf16[8,512,256]{2,1,0:T(8,128)(2,1)}), bf16[8,512,256]{2,1,0:T(8,128)(2,1)}, u32[]{:S(2)}, u32[]{:S(2)}) async-start(bf16[8,512,256]{2,1,0:T(8,128)(2,1)} %broadcast_in_dim.21), calls=%async_computation | async-start | bytes 4194304 | tf_op jit(solution)/shard_map/all_to_all | solution.py:18
  16.5 140.9 %all-gather.2.cloned.1.call-start = ((), (), s32[]{:S(2)}) async-start(), calls=%async_computation.2 | async-start | bytes 9732096 | tf_op jit(solution)/shard_map/all_gather | solution.py:40
  42.8 6.2 %copy-start.13 = (f32[2048]{0:T(1024)S(1)}, f32[2048]{0:T(1024)}, u32[]{:S(2)}) copy-start(f32[2048]{0:T(1024)} %param.16) | copy-start | bytes 24580
  46.8 2.3 copy-start.4
  49.0 0.9 copy-start.12
  49.9 1.8 copy-start.2
  50.4 1.6 copy-start.11
  50.4 1.6 copy-start.14
  51.8 1.5 copy-start.7
  51.8 2.6 copy-start.5
  54.4 1.1 copy-start.16
  55.6 1.6 copy-start.3
  55.6 1.6 copy-start.9
  56.2 1.9 copy-start.10
  58.5 6.1 %collective-permute-start.1 = (bf16[128,128]{0,1:T(8,128)(2,1)S(1)}, bf16[128,128]{0,1:T(8,128)(2,1)S(1)}, u32[]{:S(2)}, u32[]{:S(2)}) collective-permute-start(bf16[128,128]{0,1:T(8,128)(2,1)S(1)} %get-tuple-element.124), channel_id=1, source_target_pairs={{8,0},{16,8},{24,16},{32,24},{40,32},{48,40},{56,48},{64,56},{72,6... | collective-permute-start | bytes 98312 | tf_op jit(solution)/shard_map/ppermute | solution.py:53
  59.8 5.0 %collective-permute-start = (bf16[128,128]{0,1:T(8,128)(2,1)S(1)}, bf16[128,128]{0,1:T(8,128)(2,1)S(1)}, u32[]{:S(2)}, u32[]{:S(2)}) collective-permute-start(bf16[128,128]{0,1:T(8,128)(2,1)S(1)} %get-tuple-element.125), channel_id=1, source_target_pairs={{0,8},{8,16},{16,24},{24,32},{32,40},{40,48},{48,56},{56,64},{64,7... | collective-permute-start | bytes 98312 | tf_op jit(solution)/shard_map/ppermute | solution.py:51
  64.6 0.9 copy-start.15
  172.7 1.2 slice-start
  174.1 90.1 %copy-start.6 = (bf16[128,2048]{1,0:T(8,128)(2,1)S(1)}, bf16[128,2048]{1,0:T(8,128)(2,1)}, u32[]{:S(2)}) copy-start(bf16[128,2048]{1,0:T(8,128)(2,1)} %param.26) | copy-start | bytes 1572868
  264.2 1.0 copy-start.8
  266.1 37.3 %copy-start.1 = (bf16[2048,512]{1,0:T(8,128)(2,1)S(1)}, bf16[2048,512]{1,0:T(8,128)(2,1)}, u32[]{:S(2)}) copy-start(bf16[2048,512]{1,0:T(8,128)(2,1)} %param.18) | copy-start | bytes 6291460
Sparse Core Ops, SparseCore 0:
  53.3 103.9 all-gather.1
where the time goes:
time: 312 us; the launch traced here: 310 us
  waiting for transfers between devices  117 us (38%)
  local copies, waits for them, and re-layouts  57.4 us (18%)
  matrix products  52.7 us (17%)
  blocking collectives  34.7 us (11%)
  other arithmetic  19.4 us (6%)
  between operations  13.9 us (4%)
  starting transfers between devices  12.9 us (4%)
    all_gather x1, waiting for transfers between devices, sent_together(): lax.all_gather(both, axis, axis=dim, tiled=True)  91 us
    all_to_all x1, blocking collectives, summed_on_arrival(): lax.all_to_all(parts, axis, split_axis=0, concat_axis=0, tiled=True)  34.7 us
    dynamic_slice x32, local copies, waits for them, and re-layouts, attend_rows(): running, unused = lax.scan(advance, running, sliced)  31.1 us
    all_to_all x1, waiting for transfers between devices, sent_to_all(): lax.all_to_all(jnp.broadcast_to(value[None], (peers, *value.shape)), axis...  26.3 us
    dot_general x32, matrix products, attend(): jnp.einsum('hqk,khd->qhd', weights.astype(jnp.bfloat16), stacked[..., NOP...  15.8 us
    dot_general x32, matrix products, attend(): jnp.einsum('qhn,khn->hqk', queries[..., :NOPE], stacked[..., :NOPE], pref...  15.3 us
    dot_general x32, matrix products, attend(): jnp.einsum('qhr,kr->hqk', queries[..., NOPE:], rope_keys, preferred_eleme...  15.1 us
    reduce_sum x32, other arithmetic, attend(): denoms = denoms * shrink + jnp.sum(weights, axis=-1)  9.72 us
  transfers between devices with their start and end apart: 4, of which 3 were waited for; matrix products, arithmetic and copies ran while one was open for 2% of the time, Pallas kernels for 0%

commit v1 on v0

v1 whole, which is shorter than its diff:
```python
import functools
import math

import jax
import jax.numpy as jnp
import numpy as np
from jax import lax
from jax.experimental import pallas as pl
from jax.experimental.pallas import tpu as pltpu
from jax.sharding import Mesh
from jax.sharding import PartitionSpec as P


NOPE = 64
ROPE = 32
HEAD = 64
WINDOW = 128
TILE = 256
epsilon = 1e-06
LOG2E = math.log2(math.e)
LATENT_SCALE = LOG2E * (NOPE + ROPE) ** (-0.5)
WINDOW_SCALE = LOG2E * HEAD ** (-0.5)
GRANT = 12 << 20
SMALLEST = 2.0**-60
LARGEST = 2.0**100
F32 = jnp.float32
BF16 = jnp.bfloat16
VMEM = pltpu.VMEM


NT = (((1,), (1,)), ((), ()))


def dot(a, b):
    return jnp.dot(a, b, preferred_element_type=F32)


def dot_nt(a, b):
    return lax.dot_general(a, b, NT, preferred_element_type=F32)


def rotate(v, cos, sin):
    half = v.shape[0] // 2
    a, b = v[:half], v[half:]
    return jnp.concatenate([a * cos - b * sin, b * cos + a * sin], axis=0)


def params(grant=GRANT):
    return pltpu.CompilerParams(vmem_limit_bytes=grant)


def vmem(count):
    return [pl.BlockSpec(memory_space=VMEM)] * count


SMEM = pl.BlockSpec(memory_space=pltpu.SMEM)
HBM = pl.BlockSpec(memory_space=pltpu.HBM)
ANY = pl.BlockSpec(memory_space=pl.ANY)


def stage_kernel(lq_hbm, rope_hbm, wk_hbm, wv_hbm, wq_hbm, up_hbm, rows_ref, up_out, wq_ref, up_ref, sems):
    copies = [
        pltpu.make_async_copy(wq_hbm, wq_ref, sems.at[0]),
        pltpu.make_async_copy(up_hbm, up_ref, sems.at[1]),
        pltpu.make_async_copy(lq_hbm, rows_ref.at[0:192], sems.at[2]),
        pltpu.make_async_copy(rope_hbm, rows_ref.at[192:224], sems.at[3]),
        pltpu.make_async_copy(wk_hbm, rows_ref.at[224:288], sems.at[4]),
        pltpu.make_async_copy(wv_hbm, rows_ref.at[288:352], sems.at[5]),
    ]
    for copy in copies:
        copy.start()
    copies[0].wait()
    rows_ref[352:480] = wq_ref[...].T
    copies[1].wait()
    up_out[...] = up_ref[...].T
    for copy in copies[2:]:
        copy.wait()


def stage(*weights):
    return pl.pallas_call(
        stage_kernel,
        out_shape=[
            jax.ShapeDtypeStruct((480, 2048), BF16),
            jax.ShapeDtypeStruct((256, 512), BF16),
        ],
        in_specs=[HBM] * len(weights),
        out_specs=vmem(2),
        scratch_shapes=[
            VMEM((2048, 128), BF16),
            VMEM((512, 256), BF16),
            pltpu.SemaphoreType.DMA((6,)),
        ],
        compiler_params=params(),
        cost_estimate=pl.CostEstimate(flops=1 << 30, bytes_accessed=9 << 20, transcendentals=0),
        name="stage",
    )(*weights)


def project_kernel(
    place,
    x_refs,
    gain_ref,
    lgain_ref,
    rows_ref,
    up_ref,
    cos_ref,
    sin_ref,
    down_hbm,
    chunk_refs,
    wq_out,
    wkv_out,
    hid,
    down_ref,
    sem,
):
    chip, line, core = place[0], place[1], place[2]
    blocks = gain_ref.shape[0]
    width = gain_ref.shape[2]
    fetch = pltpu.make_async_copy(down_hbm, down_ref, sem)
    fetch.start()
    for part in range(2):
        at = slice(part * TILE, (part + 1) * TILE)
        pieces = []
        for ref, chips, cores, rows in x_refs:
            if rows is None:
                pieces.append((ref, at, chips, cores))
            elif rows == part:
                pieces.append((ref, slice(0, TILE), chips, cores))
        total = jnp.zeros((TILE, 1), F32)
        for ref, rows, _, _ in pieces:
            x = ref[rows].astype(F32)
            total += jnp.sum(x * x, axis=1, keepdims=True)
        scale = lax.rsqrt(total / (blocks * width) + epsilon)
        for ref, rows, chips, cores in pieces:
            block = 2 * ((chip + chips) % 4) + (core + cores) % 2
            x = ref[rows].astype(F32)
            hid[part, :, pl.ds(pl.multiple_of(block * width, width), width)] = (
                x * scale * gain_ref[block]
            ).astype(BF16)
    fetch.wait()
    for part in range(2):
        at = slice(part * TILE, (part + 1) * TILE)
        hidden = hid[part]
        cos64, sin64 = cos_ref[0:32, at], sin_ref[0:32, at]
        cos32, sin32 = cos_ref[32:48, at], sin_ref[32:48, at]
        raw = dot(hidden, down_ref[...])
        mean = jnp.mean(raw * raw, axis=1, keepdims=True)
        latent = (raw * lax.rsqrt(mean + epsilon) * lgain_ref[...]).astype(BF16)
        together = dot_nt(rows_ref[...], hidden)
        expanded = dot_nt(up_ref[...], latent).astype(BF16)
        queries = together[0:192]
        shared = rotate(together[192:224], cos32, sin32).astype(BF16)
        for h in range(2):
            base = h * (NOPE + ROPE)
            own = h * (NOPE + HEAD)
            plain = (queries[base : base + NOPE] * LATENT_SCALE).astype(BF16)
            turned = (
                rotate(queries[base + NOPE : base + NOPE + ROPE], cos32, sin32) * LATENT_SCALE
            ).astype(BF16)
            turn = (2 * h + part - line + 4) % 4
            for r, out in enumerate(chunk_refs):

                @pl.when(turn == r)
                def _():
                    out[0:64] = plain
                    out[64:96] = turned
                    out[96:160] = expanded[own : own + NOPE]
                    out[160:192] = shared
                    out[192:256] = expanded[own + NOPE : own + NOPE + HEAD]

        window_q = together[352:480]
        first = (rotate(window_q[0:64], cos64, sin64) * WINDOW_SCALE).astype(BF16)
        second = (rotate(window_q[64:128], cos64, sin64) * WINDOW_SCALE).astype(BF16)
        for n in range(2):
            cut = slice(n * WINDOW, (n + 1) * WINDOW)
            wq_out[2 * part + n, :, 0:WINDOW] = first[:, cut]
            wq_out[2 * part + n, :, WINDOW : 2 * WINDOW] = second[:, cut]
        wkv_out[0:64, at] = rotate(together[224:288], cos64, sin64).astype(BF16)
        wkv_out[64:128, at] = together[288:352].astype(BF16)


def project(place, pieces, weights, rows):
    where = [piece[1:] for piece in pieces]
    arrays = [piece[0] for piece in pieces]
    n = len(arrays)

    def kernel(place_ref, *refs):
        x_refs = [(ref, *at) for ref, at in zip(refs[:n], where)]
        inputs = refs[n : n + len(weights)]
        outs = refs[n + len(weights) :]
        project_kernel(place_ref, x_refs, *inputs, outs[:4], *outs[4:])

    return pl.pallas_call(
        kernel,
        out_shape=[jax.ShapeDtypeStruct((256, TILE), BF16)] * 4
        + [
            jax.ShapeDtypeStruct((rows // WINDOW, 64, 2 * WINDOW), BF16),
            jax.ShapeDtypeStruct((128, rows), BF16),
        ],
        in_specs=[SMEM] + vmem(n + len(weights) - 1) + [HBM],
        out_specs=vmem(6),
        scratch_shapes=[
            VMEM((2, TILE, 2048), BF16),
            VMEM((2048, 512), BF16),
            pltpu.SemaphoreType.DMA(()),
        ],
        compiler_params=params(16 << 20),
        cost_estimate=pl.CostEstimate(
            flops=2 * rows * 2048 * 1024, bytes_accessed=8 << 20, transcendentals=0
        ),
        name="project",
    )(place, *arrays, *weights)


def attend_kernel(first, last, tiles, kv_count, place, *refs):
    q_refs, refs = refs[:tiles], refs[tiles:]
    kv_refs, refs = refs[:kv_count], refs[kv_count:]
    if not first:
        total_in, sum_in, refs = refs[0], refs[1], refs[2:]
    if last:
        all_refs, refs = refs[:-7], refs[-7:]
        out_ref, total, sums, buf, held, everything, sem = refs
    else:
        total, sums, buf, held = refs
    if first:
        total[...] = jnp.zeros_like(total)
        sums[...] = jnp.zeros_like(sums)
    else:
        total[...] = total_in[...]
        sums[...] = sum_in[...]
    inner, _, keys = kv_refs[0].shape
    for n, ref in enumerate(kv_refs):
        held[n * inner : (n + 1) * inner] = ref[...]
    count = kv_count * inner

    def add(t, p, v):
        sums[t] += p.reshape(keys // 8, 8, TILE).sum(axis=0)
        total[t] += dot(v, p.astype(BF16))

    k = held[0, 0:96, :].T
    for t in range(tiles):
        buf[0, t] = dot(k, q_refs[t][0:96])

    def step(i, carry):
        for b in range(2):
            now = 2 * i + b
            k = held[jnp.minimum(now + 1, count - 1), 0:96, :].T
            v = held[now, 96:160, :]
            for t in range(tiles):
                buf[1 - b, t] = dot(k, q_refs[t][0:96])
                add(t, jnp.exp2(buf[b, t]), v)
        return carry

    lax.fori_loop(0, count // 2, step, 0)
    if not last:
        return

    columns = jnp.sum(sums[...], axis=1)
    fits = (jnp.min(columns) >= SMALLEST) & (jnp.max(columns) <= LARGEST)

    @pl.when(jnp.logical_not(fits))
    def _():
        for n, ref in enumerate(all_refs):
            copy = pltpu.make_async_copy(ref, everything.at[n * inner : (n + 1) * inner], sem)
            copy.start()
            copy.wait()
        for t in range(tiles):
            total[t] = jnp.zeros_like(total[t])
            sums[t] = jnp.zeros_like(sums[t])

            def again(b, shift, t=t):
                s = dot(everything[b, 0:96, :].T, q_refs[t][0:96])
                new = jnp.maximum(shift, jnp.max(s, axis=0, keepdims=True))
                shrink = jnp.exp2(shift - new)
                sums[t] *= shrink
                total[t] *= shrink
                add(t, jnp.exp2(s - new), everything[b, 96:160, :])
                return new

            lax.fori_loop(
                0, len(all_refs) * inner, again, jnp.full((1, TILE), -jnp.inf, F32)
            )

    for t in range(tiles):
        line = (place[3] - t + 4) % 4
        out_ref[line] = (total[t] / jnp.sum(sums[t], axis=0, keepdims=True)).astype(BF16)


def attend(place, chunks, kvs, state=None, everything=None):
    tiles = len(chunks)
    first, last = state is None, everything is not None
    inner, depth, keys = kvs[0].shape
    holds = [(tiles, HEAD, TILE), (tiles, 8, TILE)]
    spare = [
        VMEM((2, tiles, keys, TILE), F32),
        VMEM((len(kvs) * inner, depth, keys), BF16),
    ]
    args = (*chunks, *kvs) + (() if first else tuple(state))
    in_specs = [SMEM] + vmem(len(args))
    if last:
        out_shape = [jax.ShapeDtypeStruct((tiles, HEAD, TILE), BF16)]
        spare = [VMEM(s, F32) for s in holds] + spare
        spare += [
            VMEM((len(everything) * inner, depth, keys), BF16),
            pltpu.SemaphoreType.DMA(()),
        ]
        args += tuple(everything)
        in_specs += [ANY] * len(everything)
    else:
        out_shape = [jax.ShapeDtypeStruct(s, F32) for s in holds]
    work = tiles * TILE * len(kvs) * inner * keys
    return pl.pallas_call(
        functools.partial(attend_kernel, first, last, tiles, len(kvs)),
        out_shape=out_shape,
        in_specs=in_specs,
        out_specs=vmem(len(out_shape)),
        scratch_shapes=spare,
        compiler_params=params(),
        cost_estimate=pl.CostEstimate(
            flops=2 * work * 320, bytes_accessed=3 << 20, transcendentals=work
        ),
        name="attend_last" if last else "attend",
    )(place, *args)


def window_kernel(span_ref, q_ref, kv_ref, left_ref, right_ref, sink_ref, out_ref, ext):
    rows = kv_ref.shape[1]
    ext[:, 0:WINDOW] = left_ref[...]
    ext[:, WINDOW : WINDOW + rows] = kv_ref[...]
    ext[:, WINDOW + rows :] = right_ref[...]
    first_span, last_span = span_ref[0] == 0, span_ref[0] == span_ref[1] - 1
    wide = 3 * WINDOW
    key = lax.broadcasted_iota(jnp.int32, (wide, 2 * WINDOW), 0)
    lane = lax.broadcasted_iota(jnp.int32, (wide, 2 * WINDOW), 1)
    offset = key - jnp.where(lane >= WINDOW, lane - WINDOW, lane)
    near = (offset >= 0) & (offset <= 2 * WINDOW)
    side = lax.broadcasted_iota(jnp.int32, (1, 2 * WINDOW), 1)
    sink = jnp.where(side < WINDOW, sink_ref[0], sink_ref[1]) * LOG2E
    blocks = rows // WINDOW
    for n in range(blocks):
        k = ext[0:64, n * WINDOW : n * WINDOW + wide].T
        v = ext[64:128, n * WINDOW : n * WINDOW + wide]
        allowed = near
        if n == 0:
            allowed = allowed & ((key >= WINDOW) | jnp.logical_not(first_span))
        if n == blocks - 1:
            allowed = allowed & ((key < 2 * WINDOW) | jnp.logical_not(last_span))
        s = jnp.where(allowed, dot(k, q_ref[n]), -jnp.inf)
        top = jnp.maximum(jnp.max(s, axis=0, keepdims=True), sink)
        p = jnp.exp2(s - top)
        denom = jnp.sum(p, axis=0, keepdims=True) + jnp.exp2(sink - top)
        o = (dot(v, p.astype(BF16)) / denom).astype(BF16)
        out_ref[0:64, n * WINDOW : (n + 1) * WINDOW] = o[:, 0:WINDOW]
        out_ref[64:128, n * WINDOW : (n + 1) * WINDOW] = o[:, WINDOW:]


def windowed(span, q, kv, left, right, sink):
    smem = pl.BlockSpec(memory_space=pltpu.SMEM)
    vmem = pl.BlockSpec(memory_space=VMEM)
    rows = kv.shape[1]
    return pl.pallas_call(
        window_kernel,
        out_shape=jax.ShapeDtypeStruct((128, rows), BF16),
        in_specs=[smem, vmem, vmem, vmem, vmem, smem],
        out_specs=vmem,
        scratch_shapes=[VMEM((128, rows + 2 * WINDOW), BF16)],
        cost_estimate=pl.CostEstimate(
            flops=rows * 2 * 384 * 256, bytes_accessed=1 << 20, transcendentals=rows * 768
        ),
        compiler_params=params(),
        name="windowed",
    )(span, q, kv, left, right, sink)


def merge_kernel(place, keep_ref, got_ref, win_ref, wl_ref, ww_ref, *refs):
    own_refs, sib_refs, (mixed, lhs) = refs[:4], refs[4:8], refs[8:]
    chip, core = place[0], place[2]
    for ref, half in ((keep_ref, core), (got_ref, 1 - core)):
        at = pl.ds(pl.multiple_of(half * TILE, TILE), TILE)
        mixed[0:HEAD, at] = ref[0]
        mixed[HEAD : 2 * HEAD, at] = ref[1]
    lhs[:, 0:128] = mixed[...].T
    lhs[:, 128:256] = win_ref[...].T
    rows = lhs[...]
    width = own_refs[0].shape[1]
    for outs, side in ((sib_refs, 1 - core), (own_refs, core)):
        for k in (2, 1, 3, 0):
            start = (2 * ((chip + k) % 4) + side) * width
            at = pl.ds(pl.multiple_of(start, width), width)
            both = jnp.concatenate([wl_ref[:, at], ww_ref[:, at]], axis=0)
            outs[k][...] = dot(rows, both).astype(BF16)


def merge(place, keep, got, win, out_latent, out_window):
    rows = win.shape[1]
    return pl.pallas_call(
        merge_kernel,
        out_shape=[jax.ShapeDtypeStruct((rows, 256), BF16)] * 8,
        in_specs=[SMEM] + vmem(5),
        out_specs=vmem(8),
        scratch_shapes=[VMEM((128, rows), BF16), VMEM((rows, 256), BF16)],
        compiler_params=params(),
        cost_estimate=pl.CostEstimate(
            flops=2 * rows * 256 * 2048, bytes_accessed=4 << 20, transcendentals=0
        ),
        name="merge",
    )(place, keep, got, win, out_latent, out_window)


SWAP = [(0, 1), (1, 0)]


def shifted(value, axis, by):
    count = lax.axis_size(axis)
    return lax.ppermute(value, axis, [(i, (i + by) % count) for i in range(count)])


def other_core(value):
    return lax.ppermute(value, "c", SWAP)


def ring_step(value):
    count = lax.axis_size("z")
    up = [(2 * i, 2 * ((i + 1) % count)) for i in range(count)]
    down = [(2 * i + 1, 2 * ((i - 1) % count) + 1) for i in range(count)]
    return lax.ppermute(value, ("z", "c"), up + down)


def head_routes(turn):
    routes = []
    for y in range(4):
        d = (y + turn) % 4
        for c in range(2):
            routes.append((2 * y + c, 2 * (2 * c + d // 2) + d % 2))
    return routes


def shards(
    inputs,
    norm_gain,
    latent_query,
    latent_down,
    rope_down,
    latent_gain,
    latent_up,
    window_query,
    window_key,
    window_value,
    sink_logit,
    out_latent,
    out_window,
):
    rows = inputs.shape[0]
    core = lax.axis_index("c")
    line = lax.axis_index("y")
    span = lax.axis_index(("z", "y"))
    spans = lax.axis_size(("z", "y"))
    slot = 2 * (line % 2) + core
    place = jnp.stack([lax.axis_index("x"), line, core, slot]).astype(jnp.int32)

    before = shifted(inputs, "x", 1)
    after = shifted(inputs, "x", -1)
    far_low = shifted(before[:TILE], "x", 1)
    far_high = shifted(after[TILE:], "x", -1)
    held = [
        (inputs, 0, None),
        (before, 3, None),
        (after, 1, None),
        (far_low, 2, 0),
        (far_high, 2, 1),
    ]
    pieces = []
    for array, chips, part in held:
        pieces.append((array, chips, 0, part))
        pieces.append((other_core(array), chips, 1, part))

    staged = stage(
        latent_query.T,
        rope_down.T,
        window_key.T,
        window_value.T,
        window_query,
        latent_up,
    )
    powers = np.arange(0, HEAD, 2).astype(np.float64) / HEAD
    inverse = 1.0 / 10000.0**powers
    inverse = jnp.asarray(np.concatenate([inverse, inverse[::2]]), F32)
    positions = (span * rows + jnp.arange(rows)).astype(F32)
    angles = inverse[:, None] * positions[None, :]
    tables = jnp.cos(angles), jnp.sin(angles)
    *chunks, wq, wkv = project(
        place,
        pieces,
        (norm_gain.reshape(8, 1, 256), latent_gain[None], *staged, *tables, latent_down),
        rows,
    )
    mine = [lax.ppermute(c, ("y", "c"), head_routes(r)) for r, c in enumerate(chunks)]
    left = lax.ppermute(
        wkv[:, rows - WINDOW :], ("z", "y"), [(i, i + 1) for i in range(spans - 1)]
    )
    right = lax.ppermute(
        wkv[:, :WINDOW], ("z", "y"), [(i + 1, i) for i in range(spans - 1)]
    )
    where = jnp.stack([span, spans]).astype(jnp.int32)
    win = windowed(where, wq, wkv, left, right, sink_logit)

    low = jnp.stack([c[96:256] for c in mine])
    high = other_core(low)
    state = None
    seen = []
    for n in range(4):
        ring_low, ring_high = low, high
        low = ring_step(low)
        if n < 3:
            high = ring_step(high)
        blocks = [ring_low, ring_high]
        if n:
            blocks += [other_core(ring_low), other_core(ring_high)]
        state = attend(place, mine, blocks, state)
        seen += blocks
    blocks = [low, other_core(low)]
    (mixed,) = attend(place, mine, blocks, state, seen + blocks)

    back = lax.all_to_all(mixed, "y", 0, 0, tiled=True)
    pairs = back.reshape(2, 2, HEAD, TILE)
    keep = lax.dynamic_index_in_dim(pairs, core, 0, keepdims=False)
    give = lax.dynamic_index_in_dim(pairs, 1 - core, 0, keepdims=False)
    sums = merge(place, keep, other_core(give), win, out_latent, out_window)
    total = 0
    for k in (2, 1, 3, 0):
        own, sibling = sums[k], other_core(sums[4 + k])
        both = own.astype(F32) + sibling.astype(F32)
        if k:
            both = shifted(both.astype(BF16), "x", k).astype(F32)
        total = total + both
    return total.astype(BF16)


def solution(mesh):
    shape = (8, 4, 4, 2)
    torus = Mesh(mesh.devices.reshape(shape), ("z", "y", "x", "c"))
    sp, tp = ("z", "y"), ("x", "c")
    in_specs = (
        P(sp, tp),
        P(),
        P(None, tp),
        P(),
        P(),
        P(),
        P(None, tp),
        P(None, tp),
        P(None, tp),
        P(None, tp),
        P(tp),
        P(tp, None),
        P(tp, None),
    )
    return jax.shard_map(
        shards, mesh=torus, in_specs=in_specs, out_specs=P(sp, tp), check_vma=False
    )
```

time: 312 us -> 260 us (0.83)
  starting transfers between devices: 12.9 us -> 184 us
  waiting for transfers between devices: 117 us -> 20.7 us
  matrix products: 52.7 us -> 0 us
  local copies, waits for them, and re-layouts: 57.4 us -> 15.2 us
  blocking collectives: 34.7 us -> 0 us
  Pallas kernels: 0 us -> 34.3 us
  other arithmetic: 19.4 us -> 2.35 us
  between operations: 13.9 us -> 0.4 us
    all_to_all x1, starting transfers between devices: 7.41 us -> 118 us  [shards(): back = lax.all_to_all(mixed, 'y', 0, 0, tiled=True)]
    all_gather x1 -> x0, waiting for transfers between devices: 91 us -> none  [sent_together(): lax.all_gather(both, axis, axis=dim, tiled=True)]
    ppermute x2 -> x38, starting transfers between devices: 5.46 us -> 66.3 us  [the longest x7 22.8 us: ring_step(): return lax.ppermute(value, ('z', 'c'), up + down)]
    dot_general x107 -> x0, matrix products: 52.7 us -> none  [the longest x32 15.8 us: attend(): jnp.einsum('hqk,khd->qhd', weights.astype(jnp.bfloat16), stacked[..., NOP...]
    all_to_all x1 -> x0, blocking collectives: 34.7 us -> none  [summed_on_arrival(): lax.all_to_all(parts, axis, split_axis=0, concat_axis=0, tiled=True)]
    pallas_call x0 -> x9, Pallas kernels: none -> 34.3 us  [the longest x5 24.3 us: attend(): pl.pallas_call(functools.partial(attend_kernel, first, last, tiles, len(k...]
    dynamic_slice x32 -> x0, local copies, waits for them, and re-layouts: 31.1 us -> none  [attend_rows(): running, unused = lax.scan(advance, running, sliced)]
    all_to_all x1, waiting for transfers between devices: 26.3 us -> 0.01 us  [shards(): back = lax.all_to_all(mixed, 'y', 0, 0, tiled=True)]
  transfers between devices with their start and end apart: 4 -> 39, of which waited for: 3 -> 11; matrix products, arithmetic and copies ran while one was open for 2% -> 1% of each run, Pallas kernels for 0% -> 9%
where the time goes in v1:
time: 260 us; the launch traced here: 257 us
  starting transfers between devices  184 us (71%)
  Pallas kernels  34.3 us (13%)
  waiting for transfers between devices  20.7 us (8%)
  local copies, waits for them, and re-layouts  15.2 us (6%)
    all_to_all x1, starting transfers between devices, shards(): back = lax.all_to_all(mixed, 'y', 0, 0, tiled=True)  118 us
    pallas_call x5, Pallas kernels, attend(): pl.pallas_call(functools.partial(attend_kernel, first, last, tiles, len(k...  24.3 us
    ppermute x7, starting transfers between devices, ring_step(): return lax.ppermute(value, ('z', 'c'), up + down)  22.8 us
    ppermute x18, starting transfers between devices, other_core(): return lax.ppermute(value, 'c', SWAP)  15.3 us
    unnamed x42, local copies, waits for them, and re-layouts  14.3 us
    ppermute x7, starting transfers between devices, shifted(): lax.ppermute(value, axis, [(i, (i + by) % count) for i in range(count)])  11.9 us
    ppermute x4, starting transfers between devices, shards(): lax.ppermute(c, ('y', 'c'), head_routes(r))  11.6 us
    ppermute x7, waiting for transfers between devices, shifted(): lax.ppermute(value, axis, [(i, (i + by) % count) for i in range(count)])  11.5 us
  transfers between devices with their start and end apart: 39, of which 11 were waited for; matrix products, arithmetic and copies ran while one was open for 1% of the time, Pallas kernels for 9%

profile of v1, /device:TPU:1, one launch (start us, length us, event | category | flops | bytes accessed | tf_op | source)
XLA Modules:
  0.0 257.1 jit_solution(13568325616636904521)
XLA Ops:
  0.0 2.0 collective-permute-start.1
  3.3 3.1 %collective-permute-start = (bf16[512,256]{1,0:T(8,128)(2,1)}, bf16[512,256]{1,0:T(8,128)(2,1)S(1)}, u32[]{:S(2)}, u32[]{:S(2)}) collective-permute-start(bf16[512,256]{1,0:T(8,128)(2,1)} %refs_0_.1), channel_id=1, source_target_pairs={{0,1},{1,0},{2,3},{3,2},{4,5},{5,4},{6,7},{7,6},{8,9},{9,8},{10,11... | collective-permute-start | bytes 786440 | tf_op jit(solution)/shard_map/ppermute | solution.py:420
  7.3 2.0 collective-permute-start.5
  10.9 3.5 %collective-permute-start.2 = (bf16[512,256]{1,0:T(8,128)(2,1)S(1)}, bf16[512,256]{1,0:T(8,128)(2,1)}, u32[]{:S(2)}, u32[]{:S(2)}) collective-permute-start(bf16[512,256]{1,0:T(8,128)(2,1)S(1)} %collective-permute-done.1.refs_2_), channel_id=1, source_target_pairs={{0,1},{1,0},{2,3},{3,2},{4,5},{5,4},{6,7},{7,6},{8,9},{9,8},{10,11... | collective-permute-start | bytes 786440 | tf_op jit(solution)/shard_map/ppermute | solution.py:420
  15.5 1.7 collective-permute-start.6
  28.6 5.9 %project.1 = (bf16[256,256]{1,0:T(8,128)(2,1)S(1)}, bf16[256,256]{1,0:T(8,128)(2,1)S(1)}, bf16[256,256]{1,0:T(8,128)(2,1)S(1)}, bf16[256,256]{1,0:T(8,128)(2,1)S...) custom-call(s32[4]{0:T(128)S(1)} %pad_add_fusion.place_ref.place, bf16[512,256]{1,0:T(8,128)(2,1)S(1)} %copy-done.10, ...), custom_call_target="tpu_custom_call" | custom-call | flops 2147483648 | bytes 8388608 | tf_op jit(solution)/shard_map/project/pallas_call | solution.py:194
  34.5 4.6 %collective-permute-start.12 = (bf16[256,256]{1,0:T(8,128)(2,1)S(1)}, bf16[256,256]{1,0:T(8,128)(2,1)S(1)}, u32[]{:S(2)}, u32[]{:S(2)}) collective-permute-start(bf16[256,256]{1,0:T(8,128)(2,1)S(1)} %get-tuple-element.34), channel_id=1, source_target_pairs={{0,9},{1,25},{8,0},{9,16},{16,1},{17,17},{24,8},{25,24},{2,11},{3,... | collective-permute-start | bytes 393224 | tf_op jit(solution)/shard_map/ppermute | solution.py:498
  39.1 1.7 collective-permute-start.11
  40.8 1.9 collective-permute-start.10
  42.7 3.4 %collective-permute-start.9 = (bf16[256,256]{1,0:T(8,128)(2,1)S(1)}, bf16[256,256]{1,0:T(8,128)(2,1)S(1)}, u32[]{:S(2)}, u32[]{:S(2)}) collective-permute-start(bf16[256,256]{1,0:T(8,128)(2,1)S(1)} %get-tuple-element.31), channel_id=1, source_target_pairs={{0,0},{1,16},{8,1},{9,17},{16,8},{17,24},{24,9},{25,25},{2,2},{3,1... | collective-permute-start | bytes 393224 | tf_op jit(solution)/shard_map/ppermute | solution.py:498
  46.2 2.8 %collective-permute-done.9.refs_0_ = bf16[256,256]{1,0:T(8,128)(2,1)S(1)} collective-permute-done((bf16[256,256]{1,0:T(8,128)(2,1)S(1)}, bf16[256,256]{1,0:T(8,128)(2,1)S(1)}, u32[]{:S(2)}, u32[]{:S(2)}) %collective-permute-start.9) | collective-permute-done | bytes 131104 | tf_op jit(solution)/shard_map/ppermute | solution.py:498
  49.4 5.7 %collective-permute-start.13 = (bf16[4,160,256]{2,1,0:T(8,128)(2,1)S(1)}, bf16[4,160,256]{2,1,0:T(8,128)(2,1)S(1)}, u32[]{:S(2)}, u32[]{:S(2)}) collective-permute-start(bf16[4,160,256]{2,1,0:T(8,128)(2,1)S(1)} %pad_maximum_fusion.refs_4_.refs_8_), channel_id=1, source_target_pairs={{0,32},{32,64},{64,96},{96,128},{128,160},{160,192},{192,224},{224... | collective-permute-start | bytes 983048 | tf_op jit(solution)/shard_map/ppermute | solution.py:427
  56.5 2.5 collective-permute-done.13.refs_4_.refs_10_
  59.0 3.1 %collective-permute-start.14 = (bf16[4,160,256]{2,1,0:T(8,128)(2,1)S(1)}, bf16[4,160,256]{2,1,0:T(8,128)(2,1)S(1)}, u32[]{:S(2)}, u32[]{:S(2)}) collective-permute-start(bf16[4,160,256]{2,1,0:T(8,128)(2,1)S(1)} %collective-permute-done.13.refs_4_.refs_10_), channel_id=1, source_target_pairs={{0,32},{32,64},{64,96},{96,128},{128,160},{160,192},{192,224},{224... | collective-permute-start | bytes 983048 | tf_op jit(solution)/shard_map/ppermute | solution.py:427
  62.5 3.1 %collective-permute-start.20 = (bf16[4,160,256]{2,1,0:T(8,128)(2,1)S(1)}, bf16[4,160,256]{2,1,0:T(8,128)(2,1)S(1)}, u32[]{:S(2)}, u32[]{:S(2)}) collective-permute-start(bf16[4,160,256]{2,1,0:T(8,128)(2,1)S(1)} %collective-permute-done.19.refs_5_.refs_11_), channel_id=1, source_target_pairs={{0,32},{32,64},{64,96},{96,128},{128,160},{160,192},{192,224},{224... | collective-permute-start | bytes 983048 | tf_op jit(solution)/shard_map/ppermute | solution.py:427
  66.2 3.1 %collective-permute-start.15 = (bf16[4,160,256]{2,1,0:T(8,128)(2,1)S(1)}, bf16[4,160,256]{2,1,0:T(8,128)(2,1)S(1)}, u32[]{:S(2)}, u32[]{:S(2)}) collective-permute-start(bf16[4,160,256]{2,1,0:T(8,128)(2,1)S(1)} %collective-permute-done.14.refs_4_.refs_14_), channel_id=1, source_target_pairs={{0,32},{32,64},{64,96},{96,128},{128,160},{160,192},{192,224},{224... | collective-permute-start | bytes 983048 | tf_op jit(solution)/shard_map/ppermute | solution.py:427
  69.7 3.1 %collective-permute-start.21 = (bf16[4,160,256]{2,1,0:T(8,128)(2,1)S(1)}, bf16[4,160,256]{2,1,0:T(8,128)(2,1)}, u32[]{:S(2)}, u32[]{:S(2)}) collective-permute-start(bf16[4,160,256]{2,1,0:T(8,128)(2,1)S(1)} %collective-permute-done.20.refs_5_.refs_15_), channel_id=1, source_target_pairs={{0,32},{32,64},{64,96},{96,128},{128,160},{160,192},{192,224},{224... | collective-permute-start | bytes 983048 | tf_op jit(solution)/shard_map/ppermute | solution.py:427
  73.3 3.1 %collective-permute-start.16 = (bf16[4,160,256]{2,1,0:T(8,128)(2,1)S(1)}, bf16[4,160,256]{2,1,0:T(8,128)(2,1)S(1)}, u32[]{:S(2)}, u32[]{:S(2)}) collective-permute-start(bf16[4,160,256]{2,1,0:T(8,128)(2,1)S(1)} %collective-permute-done.15.refs_4_.refs_18_), channel_id=1, source_target_pairs={{0,32},{32,64},{64,96},{96,128},{128,160},{160,192},{192,224},{224... | collective-permute-start | bytes 983048 | tf_op jit(solution)/shard_map/ppermute | solution.py:427
  76.4 3.2 %attend.4 = (f32[4,64,256]{2,1,0:T(8,128)S(1)}, f32[4,8,256]{2,1,0:T(8,128)S(1)}) custom-call(s32[4]{0:T(128)S(1)} %pad_add_fusion.place_ref.place, bf16[256,256]{1,0:T(8,128)(2,1)S(1)} %collective-permute-done.9.refs_0_, bf16[256,256]{1,0:T(8,128)(2,1)S(1)} %collective-permute-done.10.refs_1_, bf16[256,256]{1,0:T(8,128)(2,1)S(1)} %collective-permute-done.11.refs_2_, ...), custom_call_target="tpu_custom_call" | custom-call | flops 1342177280 | bytes 3145728 | tf_op jit(solution)/shard_map/attend/pallas_call | solution.py:313
  80.9 5.6 %attend.5 = (f32[4,64,256]{2,1,0:T(8,128)S(1)}, f32[4,8,256]{2,1,0:T(8,128)S(1)}) custom-call(s32[4]{0:T(128)S(1)} %pad_add_fusion.place_ref.place, bf16[256,256]{1,0:T(8,128)(2,1)S(1)} %collective-permute-done.9.refs_0_, bf16[256,256]{1,0:T(8,128)(2,1)S(1)} %collective-permute-done.10.refs_1_, bf16[256,256]{1,0:T(8,128)(2,1)S(1)} %collective-permute-done.11.refs_2_, ...), custom_call_target="tpu_custom_call" | custom-call | flops 2684354560 | bytes 3145728 | tf_op jit(solution)/shard_map/attend/pallas_call | solution.py:313
  87.0 5.6 %attend.6 = (f32[4,64,256]{2,1,0:T(8,128)S(1)}, f32[4,8,256]{2,1,0:T(8,128)S(1)}) custom-call(s32[4]{0:T(128)S(1)} %pad_add_fusion.place_ref.place, bf16[256,256]{1,0:T(8,128)(2,1)S(1)} %collective-permute-done.9.refs_0_, bf16[256,256]{1,0:T(8,128)(2,1)S(1)} %collective-permute-done.10.refs_1_, bf16[256,256]{1,0:T(8,128)(2,1)S(1)} %collective-permute-done.11.refs_2_, ...), custom_call_target="tpu_custom_call" | custom-call | flops 2684354560 | bytes 3145728 | tf_op jit(solution)/shard_map/attend/pallas_call | solution.py:313
  92.6 6.0 %attend.7 = (f32[4,64,256]{2,1,0:T(8,128)S(1)}, f32[4,8,256]{2,1,0:T(8,128)S(1)}) custom-call(s32[4]{0:T(128)S(1)} %pad_add_fusion.place_ref.place, bf16[256,256]{1,0:T(8,128)(2,1)S(1)} %collective-permute-done.9.refs_0_, bf16[256,256]{1,0:T(8,128)(2,1)S(1)} %collective-permute-done.10.refs_1_, bf16[256,256]{1,0:T(8,128)(2,1)S(1)} %collective-permute-done.11.refs_2_, ...), custom_call_target="tpu_custom_call" | custom-call | flops 2684354560 | bytes 3145728 | tf_op jit(solution)/shard_map/attend/pallas_call | solution.py:313
  98.6 4.0 %attend_last.1 = bf16[4,64,256]{2,1,0:T(8,128)(2,1)} custom-call(s32[4]{0:T(128)S(1)} %pad_add_fusion.place_ref.place, bf16[256,256]{1,0:T(8,128)(2,1)S(1)} %collective-permute-done.9.refs_0_, bf16[256,256]{1,0:T(8,128)(2,1)S(1)} %collective-permute-done.10.refs_1_, bf16[256,256]{1,0:T(8,128)(2,1)S(1)} %collective-permute-done.11.refs_2_, ...), custom_call_target="tpu_custom_call" | custom-call | flops 1342177280 | bytes 3145728 | tf_op jit(solution)/shard_map/attend_last/pallas_call | solution.py:313
  102.7 117.9 %all-to-all-start = ((bf16[4,64,256]{2,1,0:T(8,128)(2,1)}), bf16[4,64,256]{2,1,0:T(8,128)(2,1)S(1)}, u32[]{:S(2)}, u32[]{:S(2)}) async-start(bf16[4,64,256]{2,1,0:T(8,128)(2,1)} %attend_last.1), calls=%async_computation | async-start | bytes 262144 | tf_op jit(solution)/shard_map/all_to_all | solution.py:525
  221.4 3.4 %collective-permute-start.29 = (bf16[128,128]{1,0:T(8,128)(2,1)S(1)}, bf16[128,128]{1,0:T(8,128)(2,1)S(1)}, u32[]{:S(2)}, u32[]{:S(2)}) collective-permute-start(bf16[128,128]{1,0:T(8,128)(2,1)S(1)} %get-tuple-element.54), channel_id=1, source_target_pairs={{0,8},{8,16},{16,24},{24,32},{32,40},{40,48},{48,56},{56,64},{64,7... | collective-permute-start | bytes 98312 | tf_op jit(solution)/shard_map/ppermute | solution.py:499
  227.4 2.0 collective-permute-done.30.right_ref
  231.2 2.0 windowed.1.win_ref
  236.6 2.4 collective-permute-start.31
  240.3 2.2 collective-permute-start.32
  242.6 2.1 collective-permute-start.34
  245.5 3.9 %collective-permute-done.32 = bf16[512,256]{1,0:T(8,128)(2,1)S(1)} collective-permute-done((bf16[512,256]{1,0:T(8,128)(2,1)S(1)}, bf16[512,256]{1,0:T(8,128)(2,1)S(1)}, u32[]{:S(2)}, u32[]{:S(2)}) %collective-permute-start.32) | collective-permute-done | bytes 262176 | tf_op jit(solution)/shard_map/ppermute | solution.py:416
  249.4 6.3 %collective-permute-done.34 = bf16[512,256]{1,0:T(8,128)(2,1)S(1)} collective-permute-done((bf16[512,256]{1,0:T(8,128)(2,1)S(1)}, bf16[512,256]{1,0:T(8,128)(2,1)S(1)}, u32[]{:S(2)}, u32[]{:S(2)}) %collective-permute-start.34) | collective-permute-done | bytes 262176 | tf_op jit(solution)/shard_map/ppermute | solution.py:416
  (114 shorter events, 33.7 us)
Async XLA Ops:
  0.0 7.3 %collective-permute-start.1 = (bf16[512,256]{1,0:T(8,128)(2,1)}, bf16[512,256]{1,0:T(8,128)(2,1)S(1)}, u32[]{:S(2)}, u32[]{:S(2)}) collective-permute-start(bf16[512,256]{1,0:T(8,128)(2,1)} %refs_0_.1), channel_id=1, source_target_pairs={{0,2},{2,4},{4,6},{6,0},{1,3},{3,5},{5,7},{7,1},{8,10},{10,12},{12... | collective-permute-start | bytes 786440 | tf_op jit(solution)/shard_map/ppermute | solution.py:416
  2.0 7.3 %collective-permute-start.3 = (bf16[512,256]{1,0:T(8,128)(2,1)}, bf16[512,256]{1,0:T(8,128)(2,1)S(1)}, u32[]{:S(2)}, u32[]{:S(2)}) collective-permute-start(bf16[512,256]{1,0:T(8,128)(2,1)} %refs_0_.1), channel_id=1, source_target_pairs={{0,6},{2,0},{4,2},{6,4},{1,7},{3,1},{5,3},{7,5},{8,14},{10,8},{12,... | collective-permute-start | bytes 786440 | tf_op jit(solution)/shard_map/ppermute | solution.py:416
  3.3 22.7 %collective-permute-start = (bf16[512,256]{1,0:T(8,128)(2,1)}, bf16[512,256]{1,0:T(8,128)(2,1)S(1)}, u32[]{:S(2)}, u32[]{:S(2)}) collective-permute-start(bf16[512,256]{1,0:T(8,128)(2,1)} %refs_0_.1), channel_id=1, source_target_pairs={{0,1},{1,0},{2,3},{3,2},{4,5},{5,4},{6,7},{7,6},{8,9},{9,8},{10,11... | collective-permute-start | bytes 786440 | tf_op jit(solution)/shard_map/ppermute | solution.py:420
  7.3 8.2 %collective-permute-start.5 = (bf16[256,256]{1,0:T(8,128)(2,1)S(1)}, bf16[256,256]{1,0:T(8,128)(2,1)S(1)}, u32[]{:S(2)}, u32[]{:S(2)}) collective-permute-start(bf16[256,256]{1,0:T(8,128)(2,1)S(1)} %slice.32), channel_id=1, source_target_pairs={{0,2},{2,4},{4,6},{6,0},{1,3},{3,5},{5,7},{7,1},{8,10},{10,12},{12... | collective-permute-start | bytes 393224 | tf_op jit(solution)/shard_map/ppermute | solution.py:416
  9.3 7.9 %collective-permute-start.7 = (bf16[256,256]{1,0:T(8,128)(2,1)S(1)}, bf16[256,256]{1,0:T(8,128)(2,1)}, u32[]{:S(2)}, u32[]{:S(2)}) collective-permute-start(bf16[256,256]{1,0:T(8,128)(2,1)S(1)} %slice.33), channel_id=1, source_target_pairs={{0,6},{2,0},{4,2},{6,4},{1,7},{3,1},{5,3},{7,5},{8,14},{10,8},{12,... | collective-permute-start | bytes 393224 | tf_op jit(solution)/shard_map/ppermute | solution.py:416
  10.9 15.1 %collective-permute-start.2 = (bf16[512,256]{1,0:T(8,128)(2,1)S(1)}, bf16[512,256]{1,0:T(8,128)(2,1)}, u32[]{:S(2)}, u32[]{:S(2)}) collective-permute-start(bf16[512,256]{1,0:T(8,128)(2,1)S(1)} %collective-permute-done.1.refs_2_), channel_id=1, source_target_pairs={{0,1},{1,0},{2,3},{3,2},{4,5},{5,4},{6,7},{7,6},{8,9},{9,8},{10,11... | collective-permute-start | bytes 786440 | tf_op jit(solution)/shard_map/ppermute | solution.py:420
  14.4 11.6 %collective-permute-start.4 = (bf16[512,256]{1,0:T(8,128)(2,1)S(1)}, bf16[512,256]{1,0:T(8,128)(2,1)}, u32[]{:S(2)}, u32[]{:S(2)}) collective-permute-start(bf16[512,256]{1,0:T(8,128)(2,1)S(1)} %collective-permute-done.3.refs_4_), channel_id=1, source_target_pairs={{0,1},{1,0},{2,3},{3,2},{4,5},{5,4},{6,7},{7,6},{8,9},{9,8},{10,11... | collective-permute-start | bytes 786440 | tf_op jit(solution)/shard_map/ppermute | solution.py:420
  15.5 10.5 %collective-permute-start.6 = (bf16[256,256]{1,0:T(8,128)(2,1)S(1)}, bf16[256,256]{1,0:T(8,128)(2,1)}, u32[]{:S(2)}, u32[]{:S(2)}) collective-permute-start(bf16[256,256]{1,0:T(8,128)(2,1)S(1)} %collective-permute-done.5.refs_6_), channel_id=1, source_target_pairs={{0,1},{1,0},{2,3},{3,2},{4,5},{5,4},{6,7},{7,6},{8,9},{9,8},{10,11... | collective-permute-start | bytes 393224 | tf_op jit(solution)/shard_map/ppermute | solution.py:420
  17.3 8.7 %collective-permute-start.8 = (bf16[256,256]{1,0:T(8,128)(2,1)}, bf16[256,256]{1,0:T(8,128)(2,1)}, u32[]{:S(2)}, u32[]{:S(2)}) collective-permute-start(bf16[256,256]{1,0:T(8,128)(2,1)} %collective-permute-done.7.refs_8_), channel_id=1, source_target_pairs={{0,1},{1,0},{2,3},{3,2},{4,5},{5,4},{6,7},{7,6},{8,9},{9,8},{10,11... | collective-permute-start | bytes 393224 | tf_op jit(solution)/shard_map/ppermute | solution.py:420
  34.5 11.7 %collective-permute-start.12 = (bf16[256,256]{1,0:T(8,128)(2,1)S(1)}, bf16[256,256]{1,0:T(8,128)(2,1)S(1)}, u32[]{:S(2)}, u32[]{:S(2)}) collective-permute-start(bf16[256,256]{1,0:T(8,128)(2,1)S(1)} %get-tuple-element.34), channel_id=1, source_target_pairs={{0,9},{1,25},{8,0},{9,16},{16,1},{17,17},{24,8},{25,24},{2,11},{3,... | collective-permute-start | bytes 393224 | tf_op jit(solution)/shard_map/ppermute | solution.py:498
  39.1 7.1 %collective-permute-start.11 = (bf16[256,256]{1,0:T(8,128)(2,1)S(1)}, bf16[256,256]{1,0:T(8,128)(2,1)S(1)}, u32[]{:S(2)}, u32[]{:S(2)}) collective-permute-start(bf16[256,256]{1,0:T(8,128)(2,1)S(1)} %get-tuple-element.33), channel_id=1, source_target_pairs={{0,8},{1,24},{8,9},{9,25},{16,0},{17,16},{24,1},{25,17},{2,10},{3,... | collective-permute-start | bytes 393224 | tf_op jit(solution)/shard_map/ppermute | solution.py:498
  42.7 6.3 %collective-permute-start.9 = (bf16[256,256]{1,0:T(8,128)(2,1)S(1)}, bf16[256,256]{1,0:T(8,128)(2,1)S(1)}, u32[]{:S(2)}, u32[]{:S(2)}) collective-permute-start(bf16[256,256]{1,0:T(8,128)(2,1)S(1)} %get-tuple-element.31), channel_id=1, source_target_pairs={{0,0},{1,16},{8,1},{9,17},{16,8},{17,24},{24,9},{25,25},{2,2},{3,1... | collective-permute-start | bytes 393224 | tf_op jit(solution)/shard_map/ppermute | solution.py:498
  49.4 9.7 %collective-permute-start.13 = (bf16[4,160,256]{2,1,0:T(8,128)(2,1)S(1)}, bf16[4,160,256]{2,1,0:T(8,128)(2,1)S(1)}, u32[]{:S(2)}, u32[]{:S(2)}) collective-permute-start(bf16[4,160,256]{2,1,0:T(8,128)(2,1)S(1)} %pad_maximum_fusion.refs_4_.refs_8_), channel_id=1, source_target_pairs={{0,32},{32,64},{64,96},{96,128},{128,160},{160,192},{192,224},{224... | collective-permute-start | bytes 983048 | tf_op jit(solution)/shard_map/ppermute | solution.py:427
  55.0 7.5 %collective-permute-start.19 = (bf16[4,160,256]{2,1,0:T(8,128)(2,1)S(1)}, bf16[4,160,256]{2,1,0:T(8,128)(2,1)S(1)}, u32[]{:S(2)}, u32[]{:S(2)}) collective-permute-start(bf16[4,160,256]{2,1,0:T(8,128)(2,1)S(1)} %collective-permute-done.18.refs_5_.refs_9_), channel_id=1, source_target_pairs={{0,32},{32,64},{64,96},{96,128},{128,160},{160,192},{192,224},{224... | collective-permute-start | bytes 983048 | tf_op jit(solution)/shard_map/ppermute | solution.py:427
  59.0 7.1 %collective-permute-start.14 = (bf16[4,160,256]{2,1,0:T(8,128)(2,1)S(1)}, bf16[4,160,256]{2,1,0:T(8,128)(2,1)S(1)}, u32[]{:S(2)}, u32[]{:S(2)}) collective-permute-start(bf16[4,160,256]{2,1,0:T(8,128)(2,1)S(1)} %collective-permute-done.13.refs_4_.refs_10_), channel_id=1, source_target_pairs={{0,32},{32,64},{64,96},{96,128},{128,160},{160,192},{192,224},{224... | collective-permute-start | bytes 983048 | tf_op jit(solution)/shard_map/ppermute | solution.py:427
  62.5 7.1 %collective-permute-start.20 = (bf16[4,160,256]{2,1,0:T(8,128)(2,1)S(1)}, bf16[4,160,256]{2,1,0:T(8,128)(2,1)S(1)}, u32[]{:S(2)}, u32[]{:S(2)}) collective-permute-start(bf16[4,160,256]{2,1,0:T(8,128)(2,1)S(1)} %collective-permute-done.19.refs_5_.refs_11_), channel_id=1, source_target_pairs={{0,32},{32,64},{64,96},{96,128},{128,160},{160,192},{192,224},{224... | collective-permute-start | bytes 983048 | tf_op jit(solution)/shard_map/ppermute | solution.py:427
  65.6 7.1 %collective-permute-start.26 = (bf16[4,160,256]{2,1,0:T(8,128)(2,1)S(1)}, bf16[4,160,256]{2,1,0:T(8,128)(2,1)S(1)}, u32[]{:S(2)}, u32[]{:S(2)}) collective-permute-start(bf16[4,160,256]{2,1,0:T(8,128)(2,1)S(1)} %collective-permute-done.13.refs_4_.refs_10_), channel_id=1, source_target_pairs={{0,1},{1,0},{2,3},{3,2},{4,5},{5,4},{6,7},{7,6},{8,9},{9,8},{10,11... | collective-permute-start | bytes 983048 | tf_op jit(solution)/shard_map/ppermute | solution.py:420
  66.2 7.2 %collective-permute-start.15 = (bf16[4,160,256]{2,1,0:T(8,128)(2,1)S(1)}, bf16[4,160,256]{2,1,0:T(8,128)(2,1)S(1)}, u32[]{:S(2)}, u32[]{:S(2)}) collective-permute-start(bf16[4,160,256]{2,1,0:T(8,128)(2,1)S(1)} %collective-permute-done.14.refs_4_.refs_14_), channel_id=1, source_target_pairs={{0,32},{32,64},{64,96},{96,128},{128,160},{160,192},{192,224},{224... | collective-permute-start | bytes 983048 | tf_op jit(solution)/shard_map/ppermute | solution.py:427
  69.3 10.3 %collective-permute-start.27 = (bf16[4,160,256]{2,1,0:T(8,128)(2,1)S(1)}, bf16[4,160,256]{2,1,0:T(8,128)(2,1)S(1)}, u32[]{:S(2)}, u32[]{:S(2)}) collective-permute-start(bf16[4,160,256]{2,1,0:T(8,128)(2,1)S(1)} %collective-permute-done.19.refs_5_.refs_11_), channel_id=1, source_target_pairs={{0,1},{1,0},{2,3},{3,2},{4,5},{5,4},{6,7},{7,6},{8,9},{9,8},{10,11... | collective-permute-start | bytes 983048 | tf_op jit(solution)/shard_map/ppermute | solution.py:420
  69.7 10.9 %collective-permute-start.21 = (bf16[4,160,256]{2,1,0:T(8,128)(2,1)S(1)}, bf16[4,160,256]{2,1,0:T(8,128)(2,1)}, u32[]{:S(2)}, u32[]{:S(2)}) collective-permute-start(bf16[4,160,256]{2,1,0:T(8,128)(2,1)S(1)} %collective-permute-done.20.refs_5_.refs_15_), channel_id=1, source_target_pairs={{0,32},{32,64},{64,96},{96,128},{128,160},{160,192},{192,224},{224... | collective-permute-start | bytes 983048 | tf_op jit(solution)/shard_map/ppermute | solution.py:427
  72.8 14.2 %collective-permute-start.24 = (bf16[4,160,256]{2,1,0:T(8,128)(2,1)S(1)}, bf16[4,160,256]{2,1,0:T(8,128)(2,1)S(1)}, u32[]{:S(2)}, u32[]{:S(2)}) collective-permute-start(bf16[4,160,256]{2,1,0:T(8,128)(2,1)S(1)} %collective-permute-done.14.refs_4_.refs_14_), channel_id=1, source_target_pairs={{0,1},{1,0},{2,3},{3,2},{4,5},{5,4},{6,7},{7,6},{8,9},{9,8},{10,11... | collective-permute-start | bytes 983048 | tf_op jit(solution)/shard_map/ppermute | solution.py:420
  72.8 14.2 %collective-permute-start.25 = (bf16[4,160,256]{2,1,0:T(8,128)(2,1)S(1)}, bf16[4,160,256]{2,1,0:T(8,128)(2,1)S(1)}, u32[]{:S(2)}, u32[]{:S(2)}) collective-permute-start(bf16[4,160,256]{2,1,0:T(8,128)(2,1)S(1)} %collective-permute-done.20.refs_5_.refs_15_), channel_id=1, source_target_pairs={{0,1},{1,0},{2,3},{3,2},{4,5},{5,4},{6,7},{7,6},{8,9},{9,8},{10,11... | collective-permute-start | bytes 983048 | tf_op jit(solution)/shard_map/ppermute | solution.py:420
  73.3 13.2 %collective-permute-start.16 = (bf16[4,160,256]{2,1,0:T(8,128)(2,1)S(1)}, bf16[4,160,256]{2,1,0:T(8,128)(2,1)S(1)}, u32[]{:S(2)}, u32[]{:S(2)}) collective-permute-start(bf16[4,160,256]{2,1,0:T(8,128)(2,1)S(1)} %collective-permute-done.15.refs_4_.refs_18_), channel_id=1, source_target_pairs={{0,32},{32,64},{64,96},{96,128},{128,160},{160,192},{192,224},{224... | collective-permute-start | bytes 983048 | tf_op jit(solution)/shard_map/ppermute | solution.py:427
  79.6 13.0 %collective-permute-start.22 = (bf16[4,160,256]{2,1,0:T(8,128)(2,1)S(1)}, bf16[4,160,256]{2,1,0:T(8,128)(2,1)S(1)}, u32[]{:S(2)}, u32[]{:S(2)}) collective-permute-start(bf16[4,160,256]{2,1,0:T(8,128)(2,1)S(1)} %collective-permute-done.15.refs_4_.refs_18_), channel_id=1, source_target_pairs={{0,1},{1,0},{2,3},{3,2},{4,5},{5,4},{6,7},{7,6},{8,9},{9,8},{10,11... | collective-permute-start | bytes 983048 | tf_op jit(solution)/shard_map/ppermute | solution.py:420
  80.6 12.0 %collective-permute-start.23 = (bf16[4,160,256]{2,1,0:T(8,128)(2,1)}, bf16[4,160,256]{2,1,0:T(8,128)(2,1)S(1)}, u32[]{:S(2)}, u32[]{:S(2)}) collective-permute-start(bf16[4,160,256]{2,1,0:T(8,128)(2,1)} %collective-permute-done.21.refs_5_.refs_19_), channel_id=1, source_target_pairs={{0,1},{1,0},{2,3},{3,2},{4,5},{5,4},{6,7},{7,6},{8,9},{9,8},{10,11... | collective-permute-start | bytes 983048 | tf_op jit(solution)/shard_map/ppermute | solution.py:420
  86.5 12.1 %collective-permute-start.17 = (bf16[4,160,256]{2,1,0:T(8,128)(2,1)S(1)}, bf16[4,160,256]{2,1,0:T(8,128)(2,1)S(1)}, u32[]{:S(2)}, u32[]{:S(2)}) collective-permute-start(bf16[4,160,256]{2,1,0:T(8,128)(2,1)S(1)} %collective-permute-done.16.refs_4_.refs_22_), channel_id=1, source_target_pairs={{0,1},{1,0},{2,3},{3,2},{4,5},{5,4},{6,7},{7,6},{8,9},{9,8},{10,11... | collective-permute-start | bytes 983048 | tf_op jit(solution)/shard_map/ppermute | solution.py:420
  102.7 123.3 %all-to-all-start = ((bf16[4,64,256]{2,1,0:T(8,128)(2,1)}), bf16[4,64,256]{2,1,0:T(8,128)(2,1)S(1)}, u32[]{:S(2)}, u32[]{:S(2)}) async-start(bf16[4,64,256]{2,1,0:T(8,128)(2,1)} %attend_last.1), calls=%async_computation | async-start | bytes 262144 | tf_op jit(solution)/shard_map/all_to_all | solution.py:525
  221.4 6.0 %collective-permute-start.29 = (bf16[128,128]{1,0:T(8,128)(2,1)S(1)}, bf16[128,128]{1,0:T(8,128)(2,1)S(1)}, u32[]{:S(2)}, u32[]{:S(2)}) collective-permute-start(bf16[128,128]{1,0:T(8,128)(2,1)S(1)} %get-tuple-element.54), channel_id=1, source_target_pairs={{0,8},{8,16},{16,24},{24,32},{32,40},{40,48},{48,56},{56,64},{64,7... | collective-permute-start | bytes 98312 | tf_op jit(solution)/shard_map/ppermute | solution.py:499
  226.1 7.2 %collective-permute-start.28 = (bf16[2,64,256]{2,1,0:T(8,128)(2,1)S(1)}, bf16[2,64,256]{2,1,0:T(8,128)(2,1)S(1)}, u32[]{:S(2)}, u32[]{:S(2)}) collective-permute-start(bf16[2,64,256]{2,1,0:T(8,128)(2,1)S(1)} %get-tuple-element.55), channel_id=1, source_target_pairs={{0,1},{1,0},{2,3},{3,2},{4,5},{5,4},{6,7},{7,6},{8,9},{9,8},{10,11... | collective-permute-start | bytes 196616 | tf_op jit(solution)/shard_map/ppermute | solution.py:420
  240.3 9.1 %collective-permute-start.32 = (bf16[512,256]{1,0:T(8,128)(2,1)S(1)}, bf16[512,256]{1,0:T(8,128)(2,1)S(1)}, u32[]{:S(2)}, u32[]{:S(2)}) collective-permute-start(bf16[512,256]{1,0:T(8,128)(2,1)S(1)} %add_convert_fusion.3), channel_id=1, source_target_pairs={{0,4},{2,6},{4,0},{6,2},{1,5},{3,7},{5,1},{7,3},{8,12},{10,14},{12... | collective-permute-start | bytes 786440 | tf_op jit(solution)/shard_map/ppermute | solution.py:416
  242.6 13.2 %collective-permute-start.34 = (bf16[512,256]{1,0:T(8,128)(2,1)S(1)}, bf16[512,256]{1,0:T(8,128)(2,1)S(1)}, u32[]{:S(2)}, u32[]{:S(2)}) collective-permute-start(bf16[512,256]{1,0:T(8,128)(2,1)S(1)} %add_convert_fusion.2), channel_id=1, source_target_pairs={{0,2},{2,4},{4,6},{6,0},{1,3},{3,5},{5,7},{7,1},{8,10},{10,12},{12... | collective-permute-start | bytes 786440 | tf_op jit(solution)/shard_map/ppermute | solution.py:416
  244.7 11.5 %collective-permute-start.36 = (bf16[512,256]{1,0:T(8,128)(2,1)S(1)}, bf16[512,256]{1,0:T(8,128)(2,1)S(1)}, u32[]{:S(2)}, u32[]{:S(2)}) collective-permute-start(bf16[512,256]{1,0:T(8,128)(2,1)S(1)} %add_convert_fusion.1), channel_id=1, source_target_pairs={{0,6},{2,0},{4,2},{6,4},{1,7},{3,1},{5,3},{7,5},{8,14},{10,8},{12,... | collective-permute-start | bytes 786440 | tf_op jit(solution)/shard_map/ppermute | solution.py:416
  (28 other events, 320.9 us)
